TPU v7x, 512 devices: a whole 4x8x8 slice. The times are simulated.
512 devices in a mesh: ep: 32 (over z, x), tp: 16 (over y, core).
Axes of the slice: x: 4, y: 8, z: 8, core: 2. Of those that a mesh axis runs over, the one named last changes fastest.
Arguments:
- query_rows: bfloat16 [16384, 3072], P('ep', 'tp'), may hold values from -6 to 6
- key_rows: bfloat16 [16384, 1024], P('ep', 'tp'), may hold values from -6 to 6
- value_rows: bfloat16 [16384, 1024], P('ep', 'tp'), may hold values from -6 to 6
- query_gain: float32 [48, 64], P('tp'), may hold values from 0.4 to 48
- key_gain: float32 [16, 64], P('tp'), may hold values from 0.1 to 1.9
- sink_logits: float32 [48], P('tp'), may hold values from 1 to 6
- out_weight: bfloat16 [3072, 2048], P('tp'), may hold values from -0.109375 to 0.109375
- expert_input: bfloat16 [16384, 2048], P(('ep', 'tp')), may hold values from -6 to 6
- expert_gain: float32 [2048], replicated, may hold values from 0.1 to 1.9
- routes: int32 [16384, 2], P(('ep', 'tp')), may hold values from 0 to 31, all different within a row; in each aligned block of 32 rows (0 to 31, 32 to 63, ...) at most 3 rows name the same one
- route_logits: float32 [16384, 2], P(('ep', 'tp')), may hold values from -6 to 6
- gate_weight: bfloat16 [32, 2048, 2048], P('ep', None, 'tp'), may hold values from -0.375 to 0.375
- up_weight: bfloat16 [32, 2048, 2048], P('ep', None, 'tp'), may hold values from -0.375 to 0.375
- down_weight: bfloat16 [32, 2048, 2048], P('ep', 'tp'), may hold values from -0.01953125 to 0.01953125
Outputs:
- attended: bfloat16 [16384, 2048], P(('ep', 'tp'))
- expert_mix: bfloat16 [16384, 2048], P(('ep', 'tp'))
Inputs may be any that keep to these rules, and one draw needn't show every extreme that they name: `routes`: each row names 2 different experts; in the rows of one device no expert is named more than 3 times, and in some device one expert is named exactly 3 times.
All inputs are finite; a program needn't handle non-finite values.
Results may differ from a plain program's by a relative error of at most 0.017.
The roundings to bfloat16 on the way count: a program that leaves them out, or rounds other values in their place, can miss the bound.
Values may be sent and summed in bfloat16 or wider, within the bound.
A program may use at most 64 MiB of HBM per device.

v0:
```python
import jax
import jax.numpy as jnp
from jax import lax
from jax.sharding import PartitionSpec as P

EXPERTS = 32
WINDOW = 128
EPSILON = 1e-06
CLAMP_LIMIT = 7.0
ACT_SLOPE = 1.702
NEGATIVE = -1e30


def shifted(value, axis, steps):
    count = lax.axis_size(axis)
    initial, last = (max(0, -steps), min(count, count - steps))
    return lax.ppermute(value, axis, [(source, source + steps) for source in range(initial, last)])


def head_norm(row_data, gain_table):
    head_count, head_size = gain_table.shape
    widened = row_data.astype(jnp.float32).reshape(row_data.shape[0], head_count, head_size)
    scaled = widened * lax.rsqrt(jnp.mean(widened * widened, axis=-1, keepdims=True) + EPSILON)
    return (scaled * gain_table).astype(jnp.bfloat16)


def band(padded, blocks):
    tiled = padded.reshape((blocks + 1, WINDOW) + padded.shape[1:])
    return jnp.concatenate([tiled[:-1], tiled[1:]], axis=1)


def attend(query_rows, key_rows, value_rows, query_gain, key_gain, sink_logits):
    seq_rows = query_rows.shape[0]
    key_heads, head_size = key_gain.shape
    group_size = query_gain.shape[0] // key_heads
    blocks = seq_rows // WINDOW
    query_hat = head_norm(query_rows, query_gain).reshape(
        blocks, WINDOW, key_heads, group_size, head_size
    )
    key_hat = head_norm(key_rows, key_gain)
    value_hat = value_rows.reshape(seq_rows, key_heads, head_size)
    tail_rows = jnp.stack([key_hat[seq_rows - WINDOW :], value_hat[seq_rows - WINDOW :]])
    earlier = shifted(tail_rows, "ep", 1)
    key_band = band(jnp.concatenate([earlier[0], key_hat], axis=0), blocks)
    value_band = band(jnp.concatenate([earlier[1], value_hat], axis=0), blocks)
    query_pos = lax.broadcasted_iota(jnp.int32, (WINDOW, 2 * WINDOW), 0)
    key_pos = lax.broadcasted_iota(jnp.int32, (WINDOW, 2 * WINDOW), 1)
    distance = query_pos + WINDOW - key_pos
    inside = (distance >= 0) & (distance < WINDOW)
    first_block = (lax.broadcasted_iota(jnp.int32, (blocks, 1, 1), 0) == 0) & (
        lax.axis_index("ep") == 0
    )
    allowed = inside[None] & ~(first_block & (key_pos < WINDOW)[None])
    scores = jnp.einsum(
        "bqkgd,bjkd->bkgqj", query_hat, key_band, preferred_element_type=jnp.float32
    ) * head_size ** (-0.5)
    scores = jnp.where(allowed[:, None, None], scores, NEGATIVE)
    sink_table = sink_logits.reshape(1, key_heads, group_size, 1, 1)
    highest = jnp.maximum(jnp.max(scores, axis=-1, keepdims=True), sink_table)
    weights = jnp.exp(scores - highest)
    total = jnp.sum(weights, axis=-1, keepdims=True) + jnp.exp(sink_table - highest)
    mixed = jnp.einsum(
        "bkgqj,bjkd->bkgqd",
        weights.astype(jnp.bfloat16),
        value_band,
        preferred_element_type=jnp.float32,
    )
    mixed = (mixed / total).astype(jnp.bfloat16)
    return jnp.transpose(mixed, (0, 3, 1, 2, 4)).reshape(seq_rows, -1)


def slot_maps(route_block, capacity):
    flat_routes = route_block.reshape(-1)
    expert_hot = (flat_routes[:, None] == lax.broadcasted_iota(jnp.int32, (1, EXPERTS), 1)).astype(
        jnp.int32
    )
    before = jnp.cumsum(expert_hot, axis=0) - expert_hot
    position = jnp.sum(before * expert_hot, axis=1)
    place_hot = (position[:, None] == lax.broadcasted_iota(jnp.int32, (1, capacity), 1)).astype(
        jnp.float32
    )
    row_total, fanout = route_block.shape
    return (
        expert_hot.astype(jnp.float32).reshape(row_total, fanout, EXPERTS),
        place_hot.reshape(row_total, fanout, capacity),
    )


def dispatch_matrix(route_block, capacity):
    expert_hot, place_hot = slot_maps(route_block, capacity)
    return jnp.einsum("rke,rkc->ecr", expert_hot, place_hot).astype(jnp.bfloat16)


def combine_matrix(route_block, route_weight, capacity):
    expert_hot, place_hot = slot_maps(route_block, capacity)
    return jnp.einsum("rke,rkc,rk->rec", expert_hot, place_hot, route_weight)


def expert_hidden(piece, gate_weight, up_weight):
    gate_pre = jnp.einsum("aecd,edf->aecf", piece, gate_weight, preferred_element_type=jnp.float32)
    up_pre = jnp.einsum("aecd,edf->aecf", piece, up_weight, preferred_element_type=jnp.float32)
    clipped = jnp.minimum(gate_pre, CLAMP_LIMIT)
    linear = jnp.clip(up_pre, -CLAMP_LIMIT, CLAMP_LIMIT)
    return (clipped * jax.nn.sigmoid(ACT_SLOPE * clipped) * (linear + 1.0)).astype(jnp.bfloat16)


def on_device(
    query_rows,
    key_rows,
    value_rows,
    query_gain,
    key_gain,
    sink_logits,
    out_weight,
    expert_input,
    expert_gain,
    routes,
    route_logits,
    gate_weight,
    up_weight,
    down_weight,
):
    heads_out = attend(query_rows, key_rows, value_rows, query_gain, key_gain, sink_logits)
    attended = lax.psum_scatter(
        jnp.dot(heads_out, out_weight, preferred_element_type=jnp.float32).astype(jnp.bfloat16),
        "tp",
        scatter_dimension=0,
        tiled=True,
    )
    own_rows = expert_input.shape[0]
    fanout = routes.shape[1]
    capacity = (3 * own_rows * fanout + 2 * EXPERTS - 1) // (2 * EXPERTS)
    ep_size = lax.axis_size("ep")
    tp_size = lax.axis_size("tp")
    local_experts = gate_weight.shape[0]
    widened = expert_input.astype(jnp.float32)
    normed = (
        widened
        * lax.rsqrt(jnp.mean(widened * widened, axis=-1, keepdims=True) + EPSILON)
        * expert_gain
    ).astype(jnp.bfloat16)
    route_weight = jax.nn.softmax(route_logits, axis=-1)
    combine = combine_matrix(routes, route_weight, capacity)
    sender = dispatch_matrix(routes, capacity)
    slot_rows = jnp.einsum(
        "ecr,rd->ecd", sender, normed, preferred_element_type=jnp.float32
    ).astype(jnp.bfloat16)
    slot_rows = slot_rows.reshape(ep_size, local_experts, capacity, -1)
    arrived = lax.all_to_all(slot_rows, "ep", split_axis=0, concat_axis=0, tiled=True)
    hidden_units = expert_hidden(
        lax.all_gather(arrived, "tp", axis=0, tiled=True), gate_weight, up_weight
    )
    partial_value = jnp.einsum(
        "aecf,efd->aecd", hidden_units, down_weight, preferred_element_type=jnp.float32
    ).astype(jnp.bfloat16)
    partial_value = partial_value.reshape(tp_size, ep_size * local_experts * capacity, -1)
    pieces = lax.all_to_all(partial_value, "tp", split_axis=0, concat_axis=0, tiled=True)
    summed = jnp.sum(pieces, axis=0, dtype=jnp.float32).astype(jnp.bfloat16)
    summed = summed.reshape(ep_size, local_experts * capacity, -1)
    returned = lax.all_to_all(summed, "ep", split_axis=0, concat_axis=0, tiled=True)
    expert_mix = jnp.einsum("rec,ecd->rd", combine, returned.astype(jnp.float32)).astype(
        jnp.bfloat16
    )
    return (attended, expert_mix)


def solution(mesh):
    placed = (
        P("ep", "tp"),
        P("ep", "tp"),
        P("ep", "tp"),
        P("tp", None),
        P("tp", None),
        P("tp"),
        P("tp", None),
        P(("ep", "tp"), None),
        P(),
        P(("ep", "tp"), None),
        P(("ep", "tp"), None),
        P("ep", None, "tp"),
        P("ep", None, "tp"),
        P("ep", "tp", None),
    )
    return jax.shard_map(
        on_device,
        mesh=mesh,
        in_specs=placed,
        out_specs=(P(("ep", "tp"), None), P(("ep", "tp"), None)),
        check_vma=False,
    )
```

profile of v0, /device:TPU:24, one launch (start us, length us, event | category | flops | bytes accessed | tf_op | source)
XLA Modules:
  0.0 328.0 jit_solution(9556012948772609825)
XLA Ops:
  7.2 1.1 fusion.58
  8.3 0.8 copy.42
  9.4 0.2 select_reduce_fusion
  9.6 0.1 eq.72
  9.7 0.4 fusion.34
  10.1 1.2 fusion.4
  11.3 0.3 copy.46
  11.6 30.7 %all_to_all.15 = bf16[32,1,3,2048]{3,2,1,0:T(4,128)(2,1)S(1)} all-to-all(bf16[32,1,3,2048]{3,2,1,0:T(4,128)(2,1)S(1)} %copy.46), channel_id=1, replica_groups=mesh['ep'=32,'tp'=16] {'ep'}, dimensions={0} | all-to-all | bytes 786432 | tf_op jit(solution)/shard_map/all_to_all | solution.py:149
  42.3 1.1 copy.47
  43.5 44.1 %all-gather.2.cloned.1.call-done = bf16[512,1,3,2048]{3,0,2,1:T(8,128)(2,1)} async-done(((bf16[32,1,3,2048]{3,0,2,1:T(8,128)(2,1)}), bf16[512,1,3,2048]{3,0,2,1:T(8,128)(2,1)}) %all-gather.2.cloned.1.call-update) | async-done | bytes 6291472 | tf_op jit(solution)/shard_map/all_gather | solution.py:151
  87.5 4.6 %fusion.11 = f32[512,1,3,128]{3,0,2,1:T(8,128)S(1)} fusion(bf16[512,1,3,2048]{3,0,2,1:T(8,128)(2,1)} %all-gather.2.cloned.1.call-done, bf16[1,2048,128]{2,1,0:T(8,128)(2,1)S(1)} %copy-done.9), kind=kOutput, calls=%fused_computation.15 | convolution fusion | flops 805502976 | bytes 7602176 | tf_op jit(solution)/shard_map/aecd,edf->aecf/dot_general | solution.py:100
  92.1 11.9 %convert_bitcast_fusion = bf16[512,1,3,2048]{3,0,2,1:T(8,128)(2,1)} fusion(bf16[512,1,3,2048]{3,0,2,1:T(8,128)(2,1)} %all-gather.2.cloned.1.call-done, f32[512,1,3,128]{3,0,2,1:T(8,128)S(1)} %fusion.11, bf16[1,128,2048]{2,1,0:T(8,128)(2,1)S(1)} %copy-done.3, bf16[1,2048,128]{2,1,0:T(8,128)(2,1)S(1)} %copy-done.4), kind=kOutput, calls=%fused_computation.4 | convolution fusion | flops 1615527936 | bytes 14417920 | tf_op jit(solution)/shard_map/aecf,efd->aecd/dot_general | solution.py:153
  104.1 11.6 %copy.48 = bf16[512,1,3,2048]{3,2,0,1:T(4,128)(2,1)} copy(bf16[512,1,3,2048]{3,0,2,1:T(8,128)(2,1)} %convert_bitcast_fusion) | data formatting | bytes 12582912 | tf_op jit(solution)/shard_map/convert_element_type | solution.py:155
  115.6 16.3 %reshape.224 = bf16[16,96,2048]{2,1,0:T(8,128)(2,1)} reshape(bf16[512,1,3,2048]{3,2,0,1:T(4,128)(2,1)} %copy.48) | data formatting | bytes 12582912 | tf_op jit(solution)/shard_map/reshape | solution.py:156
  132.0 5.5 %all-to-all-start.1 = ((bf16[16,96,2048]{2,1,0:T(8,128)(2,1)}), bf16[16,96,2048]{2,1,0:T(8,128)(2,1)}, u32[]{:S(2)}, u32[]{:S(2)}) async-start(bf16[16,96,2048]{2,1,0:T(8,128)(2,1)} %reshape.224), calls=%async_computation.2 | async-start | bytes 12582912 | tf_op jit(solution)/shard_map/all_to_all | solution.py:157
  137.7 3.4 %collective-permute-start = (bf16[2,128,1,64]{1,3,2,0:T(8,128)(2,1)S(1)}, bf16[2,128,1,64]{1,3,2,0:T(8,128)(2,1)S(1)}, u32[]{:S(2)}, u32[]{:S(2)}) collective-permute-start(bf16[2,128,1,64]{1,3,2,0:T(8,128)(2,1)S(1)} %pad_maximum_fusion.2), channel_id=1, source_target_pairs={{0,16},{16,32},{32,48},{48,64},{64,80},{80,96},{96,112},{112,128},... | collective-permute-start | bytes 98312 | tf_op jit(solution)/shard_map/ppermute | solution.py:17
  141.4 0.2 not_and_fusion
  141.6 0.1 reshape.213
  141.8 0.9 collective-permute-done
  142.7 0.5 fusion.105
  143.3 0.2 fusion.6
  143.6 0.4 fusion.33
  144.0 0.2 copy.41
  144.1 2.1 convolution_convert_fusion
  146.3 140.4 %all-to-all-done.1 = bf16[16,96,2048]{2,1,0:T(8,128)(2,1)} async-done(((bf16[16,96,2048]{2,1,0:T(8,128)(2,1)}), bf16[16,96,2048]{2,1,0:T(8,128)(2,1)}, u32[]{:S(2)}, u32[]{:S(2)}) %all-to-all-start.1) | async-done | bytes 6291488 | tf_op jit(solution)/shard_map/all_to_all | solution.py:157
  286.7 4.1 %reduce_sum.76 = bf16[96,2048]{1,0:T(8,128)(2,1)S(1)} reduce(bf16[16,96,2048]{2,1,0:T(8,128)(2,1)} %all-to-all-done.1, bf16[]{:T(256)} %constant.49.clone.1), dimensions={0}, to_apply=%region_10.11 | reduce | flops 2949120 | bytes 6684674 | tf_op jit(solution)/shard_map/reduce_sum | solution.py:158
  290.8 1.0 reshape.225
  291.8 10.2 %all-to-all-start.2 = ((bf16[32,3,2048]{2,1,0:T(4,128)(2,1)}), bf16[32,3,2048]{2,1,0:T(4,128)(2,1)S(1)}, u32[]{:S(2)}, u32[]{:S(2)}) async-start(bf16[32,3,2048]{2,1,0:T(4,128)(2,1)} %reshape.225), calls=%async_computation.3 | async-start | bytes 1048576 | tf_op jit(solution)/shard_map/all_to_all | solution.py:160
  302.0 0.1 copy.44
  302.2 0.4 fusion.84
  302.5 17.5 %all-to-all-done.2 = bf16[32,3,2048]{2,1,0:T(4,128)(2,1)S(1)} async-done(((bf16[32,3,2048]{2,1,0:T(4,128)(2,1)}), bf16[32,3,2048]{2,1,0:T(4,128)(2,1)S(1)}, u32[]{:S(2)}, u32[]{:S(2)}) %all-to-all-start.2) | async-done | bytes 393248 | tf_op jit(solution)/shard_map/all_to_all | solution.py:160
  320.1 1.1 fusion.5
  (56 shorter events, 1.1 us)
Async XLA Ops:
  7.2 137.0 %copy-start = (bf16[192,2048]{1,0:T(8,128)(2,1)S(1)}, bf16[192,2048]{1,0:T(8,128)(2,1)}, u32[]{:S(2)}) copy-start(bf16[192,2048]{1,0:T(8,128)(2,1)} %param.20) | copy-start | bytes 2359300
  7.2 80.4 %all-gather.2.cloned.1.call-start = ((), (), s32[]{:S(2)}) async-start(), calls=%async_computation.5 | async-start | bytes 6684672 | tf_op jit(solution)/shard_map/all_gather | solution.py:151
  9.7 77.9 %copy-start.9 = (bf16[1,2048,128]{2,1,0:T(8,128)(2,1)S(1)}, bf16[1,2048,128]{2,1,0:T(8,128)(2,1)}, u32[]{:S(2)}) copy-start(bf16[1,2048,128]{2,1,0:T(8,128)(2,1)} %param.25) | copy-start | bytes 1572868
  43.4 48.7 %copy-start.3 = (bf16[1,128,2048]{2,1,0:T(8,128)(2,1)S(1)}, bf16[1,128,2048]{2,1,0:T(8,128)(2,1)}, u32[]{:S(2)}) copy-start(bf16[1,128,2048]{2,1,0:T(8,128)(2,1)} %param.27) | copy-start | bytes 1572868
  43.4 48.7 %copy-start.4 = (bf16[1,2048,128]{2,1,0:T(8,128)(2,1)S(1)}, bf16[1,2048,128]{2,1,0:T(8,128)(2,1)}, u32[]{:S(2)}) copy-start(bf16[1,2048,128]{2,1,0:T(8,128)(2,1)} %param.26) | copy-start | bytes 1572868
  131.9 5.6 %copy-start.2 = (bf16[512,64]{0,1:T(8,128)(2,1)S(1)}, bf16[512,64]{0,1:T(8,128)(2,1)}, u32[]{:S(2)}) copy-start(bf16[512,64]{0,1:T(8,128)(2,1)} %param.15) | copy-start | bytes 196612
  132.0 5.6 %copy-start.7 = (f32[1,64]{1,0:T(1,128)S(1)}, f32[1,64]{1,0:T(1,128)}, u32[]{:S(2)}) copy-start(f32[1,64]{1,0:T(1,128)} %param.18) | copy-start | bytes 772
  132.0 5.7 %copy-start.5 = (bf16[512,64]{0,1:T(8,128)(2,1)S(1)}, bf16[512,64]{0,1:T(8,128)(2,1)}, u32[]{:S(2)}) copy-start(bf16[512,64]{0,1:T(8,128)(2,1)} %param.16) | copy-start | bytes 196612
  132.0 9.1 %copy-start.1 = (bf16[512,192]{0,1:T(8,128)(2,1)S(1)}, bf16[512,192]{0,1:T(8,128)(2,1)}, u32[]{:S(2)}) copy-start(bf16[512,192]{0,1:T(8,128)(2,1)} %param.14) | copy-start | bytes 589828
  132.0 154.7 %all-to-all-start.1 = ((bf16[16,96,2048]{2,1,0:T(8,128)(2,1)}), bf16[16,96,2048]{2,1,0:T(8,128)(2,1)}, u32[]{:S(2)}, u32[]{:S(2)}) async-start(bf16[16,96,2048]{2,1,0:T(8,128)(2,1)} %reshape.224), calls=%async_computation.2 | async-start | bytes 12582912 | tf_op jit(solution)/shard_map/all_to_all | solution.py:157
  137.5 5.3 %copy-start.10 = (f32[3,64]{1,0:T(4,128)S(1)}, f32[3,64]{1,0:T(4,128)}, u32[]{:S(2)}) copy-start(f32[3,64]{1,0:T(4,128)} %param.17) | copy-start | bytes 2308
  137.5 183.7 %reduce-scatter.2.cloned.1.call-start = ((), (), s32[]{:S(2)}) async-start(), calls=%async_computation.4 | async-start | bytes 2228224 | tf_op jit(solution)/shard_map/reduce_scatter | solution.py:124
  137.7 5.0 %collective-permute-start = (bf16[2,128,1,64]{1,3,2,0:T(8,128)(2,1)S(1)}, bf16[2,128,1,64]{1,3,2,0:T(8,128)(2,1)S(1)}, u32[]{:S(2)}, u32[]{:S(2)}) collective-permute-start(bf16[2,128,1,64]{1,3,2,0:T(8,128)(2,1)S(1)} %pad_maximum_fusion.2), channel_id=1, source_target_pairs={{0,16},{16,32},{32,48},{48,64},{64,80},{80,96},{96,112},{112,128},... | collective-permute-start | bytes 98312 | tf_op jit(solution)/shard_map/ppermute | solution.py:17
  141.2 2.0 copy-start.8
  146.3 155.7 %copy-start.6 = (f32[32,2]{0,1:T(2,128)S(1)}, f32[32,2]{0,1:T(2,128)}, u32[]{:S(2)}) copy-start(f32[32,2]{0,1:T(2,128)} %param.24) | copy-start | bytes 772
  291.8 28.3 %all-to-all-start.2 = ((bf16[32,3,2048]{2,1,0:T(4,128)(2,1)}), bf16[32,3,2048]{2,1,0:T(4,128)(2,1)S(1)}, u32[]{:S(2)}, u32[]{:S(2)}) async-start(bf16[32,3,2048]{2,1,0:T(4,128)(2,1)} %reshape.225), calls=%async_computation.3 | async-start | bytes 1048576 | tf_op jit(solution)/shard_map/all_to_all | solution.py:160
Sparse Core Ops, SparseCore 0:
  43.6 43.9 all-gather.1
  146.4 136.6 reduce-scatter.1
where the time goes:
time: 329 us; the launch traced here: 328 us
  waiting for transfers between devices  203 us (62%)
  local copies, waits for them, and re-layouts  31.8 us (10%)
  blocking collectives  30.7 us (9%)
  matrix products  22.5 us (7%)
  starting transfers between devices  19.1 us (6%)
  between operations  14.4 us (4%)
  other arithmetic  6.53 us (2%)
    all_to_all x1, waiting for transfers between devices, on_device(): lax.all_to_all(partial_value, 'tp', split_axis=0, concat_axis=0, tiled=True)  140 us
    all_gather x1, waiting for transfers between devices, on_device(): lax.all_gather(arrived, 'tp', axis=0, tiled=True)  44.1 us
    all_to_all x1, blocking collectives, on_device(): lax.all_to_all(slot_rows, 'ep', split_axis=0, concat_axis=0, tiled=True)  30.7 us
    all_to_all x1, waiting for transfers between devices, on_device(): lax.all_to_all(summed, 'ep', split_axis=0, concat_axis=0, tiled=True)  17.5 us
    reshape x1, local copies, waits for them, and re-layouts, on_device(): partial_value.reshape(tp_size, ep_size * local_experts * capacity, -1)  16.3 us
    dot_general x1, matrix products, on_device(): jnp.einsum('aecf,efd->aecd', hidden_units, down_weight, preferred_element...  11.9 us
    convert_element_type x1, local copies, waits for them, and re-layouts, on_device(): partial_value = jnp.einsum('aecf,efd->aecd', hidden_units, down_weight, p...  11.6 us
    all_to_all x1, starting transfers between devices, on_device(): lax.all_to_all(summed, 'ep', split_axis=0, concat_axis=0, tiled=True)  10.2 us
  transfers between devices with their start and end apart: 5, of which 4 were waited for; matrix products, arithmetic and copies ran while one was open for 3% of the time, Pallas kernels for 0%

commit v1 on v0

--- a/solution.py
+++ b/solution.py
@@ -9,6 +9,27 @@
 CLAMP_LIMIT = 7.0
 ACT_SLOPE = 1.702
 NEGATIVE = -1e30
+
+
+def collect(array, axis, dim):
+    size, index, extent = (lax.axis_size(axis), lax.axis_index(axis), array.shape[dim])
+    right = [(i, (i + 1) % size) for i in range(size)]
+    behind = [(i, (i - 1) % size) for i in range(size)]
+    filled = jnp.zeros((*array.shape[:dim], size * extent, *array.shape[dim + 1 :]), array.dtype)
+    filled = lax.dynamic_update_slice_in_dim(filled, array, index * extent, axis=dim)
+    from_left = from_right = array
+    half = size // 2
+    for step in range(1, half + 1):
+        from_left = lax.ppermute(from_left, axis, right)
+        filled = lax.dynamic_update_slice_in_dim(
+            filled, from_left, (index - step) % size * extent, axis=dim
+        )
+        if step < size - half:
+            from_right = lax.ppermute(from_right, axis, behind)
+            filled = lax.dynamic_update_slice_in_dim(
+                filled, from_right, (index + step) % size * extent, axis=dim
+            )
+    return filled
 
 
 def shifted(value, axis, steps):
@@ -147,9 +168,7 @@
     ).astype(jnp.bfloat16)
     slot_rows = slot_rows.reshape(ep_size, local_experts, capacity, -1)
     arrived = lax.all_to_all(slot_rows, "ep", split_axis=0, concat_axis=0, tiled=True)
-    hidden_units = expert_hidden(
-        lax.all_gather(arrived, "tp", axis=0, tiled=True), gate_weight, up_weight
-    )
+    hidden_units = expert_hidden(collect(arrived, "tp", 0), gate_weight, up_weight)
     partial_value = jnp.einsum(
         "aecf,efd->aecd", hidden_units, down_weight, preferred_element_type=jnp.float32
     ).astype(jnp.bfloat16)

time: 329 us -> 360 us (1.094)
  starting transfers between devices: 19.1 us -> 68.8 us
  blocking collectives: 30.7 us -> 0 us
  local copies, waits for them, and re-layouts: 31.8 us -> 39.9 us
  waiting for transfers between devices: 203 us -> 209 us
    all_gather x1 -> x0, waiting for transfers between devices: 44.1 us -> none  [on_device(): lax.all_gather(arrived, 'tp', axis=0, tiled=True)]
    ppermute x0 -> x15, waiting for transfers between devices: none -> 32.1 us  [the longest x8 32.1 us: collect(): from_left = lax.ppermute(from_left, axis, right)]
    ppermute x0 -> x15, starting transfers between devices: none -> 31.7 us  [the longest x8 28.4 us: collect(): from_left = lax.ppermute(from_left, axis, right)]
    all_to_all x1 -> x0, blocking collectives: 30.7 us -> none  [on_device(): lax.all_to_all(slot_rows, 'ep', split_axis=0, concat_axis=0, tiled=True)]
    all_to_all x0 -> x1, waiting for transfers between devices: none -> 17.5 us  [on_device(): lax.all_to_all(slot_rows, 'ep', split_axis=0, concat_axis=0, tiled=True)]
    all_to_all x0 -> x1, starting transfers between devices: none -> 13.2 us  [on_device(): lax.all_to_all(slot_rows, 'ep', split_axis=0, concat_axis=0, tiled=True)]
    all_to_all x1, starting transfers between devices: 5.5 us -> 16.5 us  [on_device(): lax.all_to_all(partial_value, 'tp', split_axis=0, concat_axis=0, tiled=True)]
    all_to_all x1, starting transfers between devices: 10.2 us -> 4.64 us  [on_device(): lax.all_to_all(summed, 'ep', split_axis=0, concat_axis=0, tiled=True)]
  transfers between devices with their start and end apart: 5 -> 20, of which waited for: 4 -> 12; matrix products, arithmetic and copies ran while one was open for 3% -> 5% of each run, Pallas kernels for 0% -> 0%
where the time goes in v1:
time: 360 us; the launch traced here: 359 us
  waiting for transfers between devices  209 us (58%)
  starting transfers between devices  68.8 us (19%)
  local copies, waits for them, and re-layouts  39.9 us (11%)
  matrix products  19.9 us (6%)
  between operations  14.9 us (4%)
  other arithmetic  6.46 us (2%)
    all_to_all x1, waiting for transfers between devices, on_device(): lax.all_to_all(partial_value, 'tp', split_axis=0, concat_axis=0, tiled=True)  141 us
    ppermute x8, waiting for transfers between devices, collect(): from_left = lax.ppermute(from_left, axis, right)  32.1 us
    ppermute x8, starting transfers between devices, collect(): from_left = lax.ppermute(from_left, axis, right)  28.4 us
    all_to_all x1, waiting for transfers between devices, on_device(): lax.all_to_all(summed, 'ep', split_axis=0, concat_axis=0, tiled=True)  17.5 us
    all_to_all x1, waiting for transfers between devices, on_device(): lax.all_to_all(slot_rows, 'ep', split_axis=0, concat_axis=0, tiled=True)  17.5 us
    all_to_all x1, starting transfers between devices, on_device(): lax.all_to_all(partial_value, 'tp', split_axis=0, concat_axis=0, tiled=True)  16.5 us
    reshape x1, local copies, waits for them, and re-layouts, on_device(): partial_value.reshape(tp_size, ep_size * local_experts * capacity, -1)  16.3 us
    all_to_all x1, starting transfers between devices, on_device(): lax.all_to_all(slot_rows, 'ep', split_axis=0, concat_axis=0, tiled=True)  13.2 us
  transfers between devices with their start and end apart: 20, of which 12 were waited for; matrix products, arithmetic and copies ran while one was open for 5% of the time, Pallas kernels for 0%

profile of v1, /device:TPU:24, one launch (start us, length us, event | category | flops | bytes accessed | tf_op | source)
XLA Modules:
  0.0 359.0 jit_solution(12004405431145661923)
XLA Ops:
  10.0 1.2 fusion
  11.2 1.1 copy.46
  12.4 13.2 %all-to-all-start = ((bf16[32,1,3,2048]{3,2,1,0:T(4,128)(2,1)}), bf16[32,1,3,2048]{3,2,1,0:T(4,128)(2,1)S(1)}, u32[]{:S(2)}, u32[]{:S(2)}) async-start(bf16[32,1,3,2048]{3,2,1,0:T(4,128)(2,1)} %copy.46), calls=%async_computation.1 | async-start | bytes 1048576 | tf_op jit(solution)/shard_map/all_to_all | solution.py:170
  25.8 17.5 %all-to-all-done = bf16[32,1,3,2048]{3,2,1,0:T(4,128)(2,1)S(1)} async-done(((bf16[32,1,3,2048]{3,2,1,0:T(4,128)(2,1)}), bf16[32,1,3,2048]{3,2,1,0:T(4,128)(2,1)S(1)}, u32[]{:S(2)}, u32[]{:S(2)}) %all-to-all-start) | async-done | bytes 393248 | tf_op jit(solution)/shard_map/all_to_all | solution.py:170
  43.3 1.7 collective-permute-start.2
  46.2 5.8 %collective-permute-done.1 = bf16[32,1,3,2048]{3,2,1,0:T(4,128)(2,1)S(1)} collective-permute-done((bf16[32,1,3,2048]{3,2,1,0:T(4,128)(2,1)S(1)}, bf16[32,1,3,2048]{3,2,1,0:T(4,128)(2,1)S(1)}, u32[]{:S(2)}, u32[]{:S(2)}) %collective-permute-start.1) | collective-permute-done | bytes 393248 | tf_op jit(solution)/shard_map/ppermute | solution.py:23
  52.7 1.3 collective-permute-start.4
  54.3 6.2 %collective-permute-done.3 = bf16[32,1,3,2048]{3,2,1,0:T(4,128)(2,1)S(1)} collective-permute-done((bf16[32,1,3,2048]{3,2,1,0:T(4,128)(2,1)S(1)}, bf16[32,1,3,2048]{3,2,1,0:T(4,128)(2,1)S(1)}, u32[]{:S(2)}, u32[]{:S(2)}) %collective-permute-start.3) | collective-permute-done | bytes 393248 | tf_op jit(solution)/shard_map/ppermute | solution.py:23
  60.5 1.6 collective-permute-start.5
  62.9 6.2 %collective-permute-done.5 = bf16[32,1,3,2048]{3,2,1,0:T(4,128)(2,1)S(1)} collective-permute-done((bf16[32,1,3,2048]{3,2,1,0:T(4,128)(2,1)S(1)}, bf16[32,1,3,2048]{3,2,1,0:T(4,128)(2,1)S(1)}, u32[]{:S(2)}, u32[]{:S(2)}) %collective-permute-start.5) | collective-permute-done | bytes 393248 | tf_op jit(solution)/shard_map/ppermute | solution.py:23
  69.1 2.8 collective-permute-start.7
  72.6 5.1 %collective-permute-done.7 = bf16[32,1,3,2048]{3,2,1,0:T(4,128)(2,1)S(1)} collective-permute-done((bf16[32,1,3,2048]{3,2,1,0:T(4,128)(2,1)S(1)}, bf16[32,1,3,2048]{3,2,1,0:T(4,128)(2,1)S(1)}, u32[]{:S(2)}, u32[]{:S(2)}) %collective-permute-start.7) | collective-permute-done | bytes 393248 | tf_op jit(solution)/shard_map/ppermute | solution.py:23
  77.7 4.1 %collective-permute-start.9 = (bf16[32,1,3,2048]{3,2,1,0:T(4,128)(2,1)S(1)}, bf16[32,1,3,2048]{3,2,1,0:T(4,128)(2,1)S(1)}, u32[]{:S(2)}, u32[]{:S(2)}) collective-permute-start(bf16[32,1,3,2048]{3,2,1,0:T(4,128)(2,1)S(1)} %collective-permute-done.7), channel_id=1, source_target_pairs={{0,1},{1,2},{2,3},{3,4},{4,5},{5,6},{6,7},{7,8},{8,9},{9,10},{10,1... | collective-permute-start | bytes 1179656 | tf_op jit(solution)/shard_map/ppermute | solution.py:23
  82.5 3.9 %collective-permute-done.9 = bf16[32,1,3,2048]{3,2,1,0:T(4,128)(2,1)S(1)} collective-permute-done((bf16[32,1,3,2048]{3,2,1,0:T(4,128)(2,1)S(1)}, bf16[32,1,3,2048]{3,2,1,0:T(4,128)(2,1)S(1)}, u32[]{:S(2)}, u32[]{:S(2)}) %collective-permute-start.9) | collective-permute-done | bytes 393248 | tf_op jit(solution)/shard_map/ppermute | solution.py:23
  86.3 5.3 %collective-permute-start.11 = (bf16[32,1,3,2048]{3,2,1,0:T(4,128)(2,1)S(1)}, bf16[32,1,3,2048]{3,2,1,0:T(4,128)(2,1)S(1)}, u32[]{:S(2)}, u32[]{:S(2)}) collective-permute-start(bf16[32,1,3,2048]{3,2,1,0:T(4,128)(2,1)S(1)} %collective-permute-done.9), channel_id=1, source_target_pairs={{0,1},{1,2},{2,3},{3,4},{4,5},{5,6},{6,7},{7,8},{8,9},{9,10},{10,1... | collective-permute-start | bytes 1179656 | tf_op jit(solution)/shard_map/ppermute | solution.py:23
  92.3 2.6 collective-permute-done.11
  94.9 6.5 %collective-permute-start.13 = (bf16[32,1,3,2048]{3,2,1,0:T(4,128)(2,1)S(1)}, bf16[32,1,3,2048]{3,2,1,0:T(4,128)(2,1)S(1)}, u32[]{:S(2)}, u32[]{:S(2)}) collective-permute-start(bf16[32,1,3,2048]{3,2,1,0:T(4,128)(2,1)S(1)} %collective-permute-done.11), channel_id=1, source_target_pairs={{0,1},{1,2},{2,3},{3,4},{4,5},{5,6},{6,7},{7,8},{8,9},{9,10},{10,1... | collective-permute-start | bytes 1179656 | tf_op jit(solution)/shard_map/ppermute | solution.py:23
  102.1 1.5 collective-permute-done.13
  103.5 7.7 %collective-permute-start.15 = (bf16[32,1,3,2048]{3,2,1,0:T(4,128)(2,1)S(1)}, bf16[32,1,3,2048]{3,2,1,0:T(4,128)(2,1)S(1)}, u32[]{:S(2)}, u32[]{:S(2)}) collective-permute-start(bf16[32,1,3,2048]{3,2,1,0:T(4,128)(2,1)S(1)} %collective-permute-done.13), channel_id=1, source_target_pairs={{0,1},{1,2},{2,3},{3,4},{4,5},{5,6},{6,7},{7,8},{8,9},{9,10},{10,1... | collective-permute-start | bytes 1179656 | tf_op jit(solution)/shard_map/ppermute | solution.py:23
  113.1 2.6 copy-done.1
  115.7 1.8 fusion.4
  117.6 12.1 %convert_bitcast_fusion = bf16[512,1,3,2048]{3,0,2,1:T(8,128)(2,1)} fusion(bf16[1,128,2048]{2,1,0:T(8,128)(2,1)S(1)} %copy-done.4, bf16[512,3,2048]{2,0,1:T(8,128)(2,1)} %copy-done.1, bf16[1,2048,128]{2,1,0:T(8,128)(2,1)S(1)} %copy-done.5, f32[512,1,3,128]{3,0,2,1:T(8,128)S(1)} %fusion.4), kind=kOutput, calls=%fused_computation | convolution fusion | flops 1615527936 | bytes 14417920 | tf_op jit(solution)/shard_map/aecf,efd->aecd/dot_general | solution.py:172
  129.7 11.4 %copy.63 = bf16[512,1,3,2048]{3,2,0,1:T(4,128)(2,1)} copy(bf16[512,1,3,2048]{3,0,2,1:T(8,128)(2,1)} %convert_bitcast_fusion) | data formatting | bytes 12582912 | tf_op jit(solution)/shard_map/convert_element_type | solution.py:174
  141.1 16.3 %reshape.301 = bf16[16,96,2048]{2,1,0:T(8,128)(2,1)} reshape(bf16[512,1,3,2048]{3,2,0,1:T(4,128)(2,1)} %copy.63) | data formatting | bytes 12582912 | tf_op jit(solution)/shard_map/reshape | solution.py:175
  157.4 16.5 %all-to-all-start.1 = ((bf16[16,96,2048]{2,1,0:T(8,128)(2,1)}), bf16[16,96,2048]{2,1,0:T(8,128)(2,1)}, u32[]{:S(2)}, u32[]{:S(2)}) async-start(bf16[16,96,2048]{2,1,0:T(8,128)(2,1)} %reshape.301), calls=%async_computation.2 | async-start | bytes 12582912 | tf_op jit(solution)/shard_map/all_to_all | solution.py:176
  174.2 2.8 collective-permute-start
  180.1 2.1 convolution_convert_fusion
  182.2 141.0 %all-to-all-done.1 = bf16[16,96,2048]{2,1,0:T(8,128)(2,1)} async-done(((bf16[16,96,2048]{2,1,0:T(8,128)(2,1)}), bf16[16,96,2048]{2,1,0:T(8,128)(2,1)}, u32[]{:S(2)}, u32[]{:S(2)}) %all-to-all-start.1) | async-done | bytes 6291488 | tf_op jit(solution)/shard_map/all_to_all | solution.py:176
  323.2 4.1 %reduce_sum.76 = bf16[96,2048]{1,0:T(8,128)(2,1)S(1)} reduce(bf16[16,96,2048]{2,1,0:T(8,128)(2,1)} %all-to-all-done.1, bf16[]{:T(256)} %constant.147.clone.1), dimensions={0}, to_apply=%region_10.11 | reduce | flops 2949120 | bytes 6684674 | tf_op jit(solution)/shard_map/reduce_sum | solution.py:177
  328.3 4.6 %all-to-all-start.2 = ((bf16[32,3,2048]{2,1,0:T(4,128)(2,1)}), bf16[32,3,2048]{2,1,0:T(4,128)(2,1)S(1)}, u32[]{:S(2)}, u32[]{:S(2)}) async-start(bf16[32,3,2048]{2,1,0:T(4,128)(2,1)} %reshape.302), calls=%async_computation.3 | async-start | bytes 1048576 | tf_op jit(solution)/shard_map/all_to_all | solution.py:179
  333.5 17.5 %all-to-all-done.2 = bf16[32,3,2048]{2,1,0:T(4,128)(2,1)S(1)} async-done(((bf16[32,3,2048]{2,1,0:T(4,128)(2,1)}), bf16[32,3,2048]{2,1,0:T(4,128)(2,1)S(1)}, u32[]{:S(2)}, u32[]{:S(2)}) %all-to-all-start.2) | async-done | bytes 393248 | tf_op jit(solution)/shard_map/all_to_all | solution.py:179
  351.0 1.1 fusion.1
  (102 shorter events, 14.8 us)
Async XLA Ops:
  7.2 172.9 %copy-start = (bf16[192,2048]{1,0:T(8,128)(2,1)S(1)}, bf16[192,2048]{1,0:T(8,128)(2,1)}, u32[]{:S(2)}) copy-start(bf16[192,2048]{1,0:T(8,128)(2,1)} %param.20) | copy-start | bytes 2359300
  12.4 30.9 %all-to-all-start = ((bf16[32,1,3,2048]{3,2,1,0:T(4,128)(2,1)}), bf16[32,1,3,2048]{3,2,1,0:T(4,128)(2,1)S(1)}, u32[]{:S(2)}, u32[]{:S(2)}) async-start(bf16[32,1,3,2048]{3,2,1,0:T(4,128)(2,1)} %copy.46), calls=%async_computation.1 | async-start | bytes 1048576 | tf_op jit(solution)/shard_map/all_to_all | solution.py:170
  43.3 8.6 %collective-permute-start.1 = (bf16[32,1,3,2048]{3,2,1,0:T(4,128)(2,1)S(1)}, bf16[32,1,3,2048]{3,2,1,0:T(4,128)(2,1)S(1)}, u32[]{:S(2)}, u32[]{:S(2)}) collective-permute-start(bf16[32,1,3,2048]{3,2,1,0:T(4,128)(2,1)S(1)} %all-to-all-done), channel_id=1, source_target_pairs={{0,1},{1,2},{2,3},{3,4},{4,5},{5,6},{6,7},{7,8},{8,9},{9,10},{10,1... | collective-permute-start | bytes 1179656 | tf_op jit(solution)/shard_map/ppermute | solution.py:23
  43.3 9.3 %collective-permute-start.2 = (bf16[32,1,3,2048]{3,2,1,0:T(4,128)(2,1)S(1)}, bf16[32,1,3,2048]{3,2,1,0:T(4,128)(2,1)S(1)}, u32[]{:S(2)}, u32[]{:S(2)}) collective-permute-start(bf16[32,1,3,2048]{3,2,1,0:T(4,128)(2,1)S(1)} %all-to-all-done), channel_id=1, source_target_pairs={{0,15},{1,0},{2,1},{3,2},{4,3},{5,4},{6,5},{7,6},{8,7},{9,8},{10,9... | collective-permute-start | bytes 1179656 | tf_op jit(solution)/shard_map/ppermute | solution.py:28
  51.9 8.6 %collective-permute-start.3 = (bf16[32,1,3,2048]{3,2,1,0:T(4,128)(2,1)S(1)}, bf16[32,1,3,2048]{3,2,1,0:T(4,128)(2,1)S(1)}, u32[]{:S(2)}, u32[]{:S(2)}) collective-permute-start(bf16[32,1,3,2048]{3,2,1,0:T(4,128)(2,1)S(1)} %collective-permute-done.1), channel_id=1, source_target_pairs={{0,1},{1,2},{2,3},{3,4},{4,5},{5,6},{6,7},{7,8},{8,9},{9,10},{10,1... | collective-permute-start | bytes 1179656 | tf_op jit(solution)/shard_map/ppermute | solution.py:23
  52.7 9.8 %collective-permute-start.4 = (bf16[32,1,3,2048]{3,2,1,0:T(4,128)(2,1)S(1)}, bf16[32,1,3,2048]{3,2,1,0:T(4,128)(2,1)S(1)}, u32[]{:S(2)}, u32[]{:S(2)}) collective-permute-start(bf16[32,1,3,2048]{3,2,1,0:T(4,128)(2,1)S(1)} %collective-permute-done.2), channel_id=1, source_target_pairs={{0,15},{1,0},{2,1},{3,2},{4,3},{5,4},{6,5},{7,6},{8,7},{9,8},{10,9... | collective-permute-start | bytes 1179656 | tf_op jit(solution)/shard_map/ppermute | solution.py:28
  54.0 61.8 %copy-start.10 = (bf16[1,2048,128]{2,1,0:T(8,128)(2,1)S(1)}, bf16[1,2048,128]{2,1,0:T(8,128)(2,1)}, u32[]{:S(2)}) copy-start(bf16[1,2048,128]{2,1,0:T(8,128)(2,1)} %param.25) | copy-start | bytes 1572868
  60.5 8.6 %collective-permute-start.5 = (bf16[32,1,3,2048]{3,2,1,0:T(4,128)(2,1)S(1)}, bf16[32,1,3,2048]{3,2,1,0:T(4,128)(2,1)S(1)}, u32[]{:S(2)}, u32[]{:S(2)}) collective-permute-start(bf16[32,1,3,2048]{3,2,1,0:T(4,128)(2,1)S(1)} %collective-permute-done.3), channel_id=1, source_target_pairs={{0,1},{1,2},{2,3},{3,4},{4,5},{5,6},{6,7},{7,8},{8,9},{9,10},{10,1... | collective-permute-start | bytes 1179656 | tf_op jit(solution)/shard_map/ppermute | solution.py:23
  62.5 9.8 %collective-permute-start.6 = (bf16[32,1,3,2048]{3,2,1,0:T(4,128)(2,1)S(1)}, bf16[32,1,3,2048]{3,2,1,0:T(4,128)(2,1)S(1)}, u32[]{:S(2)}, u32[]{:S(2)}) collective-permute-start(bf16[32,1,3,2048]{3,2,1,0:T(4,128)(2,1)S(1)} %collective-permute-done.4), channel_id=1, source_target_pairs={{0,15},{1,0},{2,1},{3,2},{4,3},{5,4},{6,5},{7,6},{8,7},{9,8},{10,9... | collective-permute-start | bytes 1179656 | tf_op jit(solution)/shard_map/ppermute | solution.py:28
  69.1 8.6 %collective-permute-start.7 = (bf16[32,1,3,2048]{3,2,1,0:T(4,128)(2,1)S(1)}, bf16[32,1,3,2048]{3,2,1,0:T(4,128)(2,1)S(1)}, u32[]{:S(2)}, u32[]{:S(2)}) collective-permute-start(bf16[32,1,3,2048]{3,2,1,0:T(4,128)(2,1)S(1)} %collective-permute-done.5), channel_id=1, source_target_pairs={{0,1},{1,2},{2,3},{3,4},{4,5},{5,6},{6,7},{7,8},{8,9},{9,10},{10,1... | collective-permute-start | bytes 1179656 | tf_op jit(solution)/shard_map/ppermute | solution.py:23
  72.3 9.8 %collective-permute-start.8 = (bf16[32,1,3,2048]{3,2,1,0:T(4,128)(2,1)S(1)}, bf16[32,1,3,2048]{3,2,1,0:T(4,128)(2,1)S(1)}, u32[]{:S(2)}, u32[]{:S(2)}) collective-permute-start(bf16[32,1,3,2048]{3,2,1,0:T(4,128)(2,1)S(1)} %collective-permute-done.6), channel_id=1, source_target_pairs={{0,15},{1,0},{2,1},{3,2},{4,3},{5,4},{6,5},{7,6},{8,7},{9,8},{10,9... | collective-permute-start | bytes 1179656 | tf_op jit(solution)/shard_map/ppermute | solution.py:28
  77.7 8.6 %collective-permute-start.9 = (bf16[32,1,3,2048]{3,2,1,0:T(4,128)(2,1)S(1)}, bf16[32,1,3,2048]{3,2,1,0:T(4,128)(2,1)S(1)}, u32[]{:S(2)}, u32[]{:S(2)}) collective-permute-start(bf16[32,1,3,2048]{3,2,1,0:T(4,128)(2,1)S(1)} %collective-permute-done.7), channel_id=1, source_target_pairs={{0,1},{1,2},{2,3},{3,4},{4,5},{5,6},{6,7},{7,8},{8,9},{9,10},{10,1... | collective-permute-start | bytes 1179656 | tf_op jit(solution)/shard_map/ppermute | solution.py:23
  82.1 9.8 %collective-permute-start.10 = (bf16[32,1,3,2048]{3,2,1,0:T(4,128)(2,1)S(1)}, bf16[32,1,3,2048]{3,2,1,0:T(4,128)(2,1)S(1)}, u32[]{:S(2)}, u32[]{:S(2)}) collective-permute-start(bf16[32,1,3,2048]{3,2,1,0:T(4,128)(2,1)S(1)} %collective-permute-done.8), channel_id=1, source_target_pairs={{0,15},{1,0},{2,1},{3,2},{4,3},{5,4},{6,5},{7,6},{8,7},{9,8},{10,9... | collective-permute-start | bytes 1179656 | tf_op jit(solution)/shard_map/ppermute | solution.py:28
  86.3 8.6 %collective-permute-start.11 = (bf16[32,1,3,2048]{3,2,1,0:T(4,128)(2,1)S(1)}, bf16[32,1,3,2048]{3,2,1,0:T(4,128)(2,1)S(1)}, u32[]{:S(2)}, u32[]{:S(2)}) collective-permute-start(bf16[32,1,3,2048]{3,2,1,0:T(4,128)(2,1)S(1)} %collective-permute-done.9), channel_id=1, source_target_pairs={{0,1},{1,2},{2,3},{3,4},{4,5},{5,6},{6,7},{7,8},{8,9},{9,10},{10,1... | collective-permute-start | bytes 1179656 | tf_op jit(solution)/shard_map/ppermute | solution.py:23
  91.9 9.8 %collective-permute-start.12 = (bf16[32,1,3,2048]{3,2,1,0:T(4,128)(2,1)S(1)}, bf16[32,1,3,2048]{3,2,1,0:T(4,128)(2,1)S(1)}, u32[]{:S(2)}, u32[]{:S(2)}) collective-permute-start(bf16[32,1,3,2048]{3,2,1,0:T(4,128)(2,1)S(1)} %collective-permute-done.10), channel_id=1, source_target_pairs={{0,15},{1,0},{2,1},{3,2},{4,3},{5,4},{6,5},{7,6},{8,7},{9,8},{10,9... | collective-permute-start | bytes 1179656 | tf_op jit(solution)/shard_map/ppermute | solution.py:28
  92.3 25.3 %copy-start.4 = (bf16[1,128,2048]{2,1,0:T(8,128)(2,1)S(1)}, bf16[1,128,2048]{2,1,0:T(8,128)(2,1)}, u32[]{:S(2)}) copy-start(bf16[1,128,2048]{2,1,0:T(8,128)(2,1)} %param.27) | copy-start | bytes 1572868
  92.3 25.3 %copy-start.5 = (bf16[1,2048,128]{2,1,0:T(8,128)(2,1)S(1)}, bf16[1,2048,128]{2,1,0:T(8,128)(2,1)}, u32[]{:S(2)}) copy-start(bf16[1,2048,128]{2,1,0:T(8,128)(2,1)} %param.26) | copy-start | bytes 1572868
  94.9 8.6 %collective-permute-start.13 = (bf16[32,1,3,2048]{3,2,1,0:T(4,128)(2,1)S(1)}, bf16[32,1,3,2048]{3,2,1,0:T(4,128)(2,1)S(1)}, u32[]{:S(2)}, u32[]{:S(2)}) collective-permute-start(bf16[32,1,3,2048]{3,2,1,0:T(4,128)(2,1)S(1)} %collective-permute-done.11), channel_id=1, source_target_pairs={{0,1},{1,2},{2,3},{3,4},{4,5},{5,6},{6,7},{7,8},{8,9},{9,10},{10,1... | collective-permute-start | bytes 1179656 | tf_op jit(solution)/shard_map/ppermute | solution.py:23
  101.7 9.8 %collective-permute-start.14 = (bf16[32,1,3,2048]{3,2,1,0:T(4,128)(2,1)S(1)}, bf16[32,1,3,2048]{3,2,1,0:T(4,128)(2,1)S(1)}, u32[]{:S(2)}, u32[]{:S(2)}) collective-permute-start(bf16[32,1,3,2048]{3,2,1,0:T(4,128)(2,1)S(1)} %collective-permute-done.12), channel_id=1, source_target_pairs={{0,15},{1,0},{2,1},{3,2},{4,3},{5,4},{6,5},{7,6},{8,7},{9,8},{10,9... | collective-permute-start | bytes 1179656 | tf_op jit(solution)/shard_map/ppermute | solution.py:28
  103.5 9.2 %collective-permute-start.15 = (bf16[32,1,3,2048]{3,2,1,0:T(4,128)(2,1)S(1)}, bf16[32,1,3,2048]{3,2,1,0:T(4,128)(2,1)S(1)}, u32[]{:S(2)}, u32[]{:S(2)}) collective-permute-start(bf16[32,1,3,2048]{3,2,1,0:T(4,128)(2,1)S(1)} %collective-permute-done.13), channel_id=1, source_target_pairs={{0,1},{1,2},{2,3},{3,4},{4,5},{5,6},{6,7},{7,8},{8,9},{9,10},{10,1... | collective-permute-start | bytes 1179656 | tf_op jit(solution)/shard_map/ppermute | solution.py:23
  113.1 2.7 copy-start.1
  157.4 16.6 %copy-start.3 = (bf16[512,64]{0,1:T(8,128)(2,1)S(1)}, bf16[512,64]{0,1:T(8,128)(2,1)}, u32[]{:S(2)}) copy-start(bf16[512,64]{0,1:T(8,128)(2,1)} %param.15) | copy-start | bytes 196612
  157.4 16.7 %copy-start.8 = (f32[1,64]{1,0:T(1,128)S(1)}, f32[1,64]{1,0:T(1,128)}, u32[]{:S(2)}) copy-start(f32[1,64]{1,0:T(1,128)} %param.18) | copy-start | bytes 772
  157.4 16.8 %copy-start.6 = (bf16[512,64]{0,1:T(8,128)(2,1)S(1)}, bf16[512,64]{0,1:T(8,128)(2,1)}, u32[]{:S(2)}) copy-start(bf16[512,64]{0,1:T(8,128)(2,1)} %param.16) | copy-start | bytes 196612
  157.4 19.6 %copy-start.2 = (bf16[512,192]{0,1:T(8,128)(2,1)S(1)}, bf16[512,192]{0,1:T(8,128)(2,1)}, u32[]{:S(2)}) copy-start(bf16[512,192]{0,1:T(8,128)(2,1)} %param.14) | copy-start | bytes 589828
  157.4 21.2 %copy-start.11 = (f32[3,64]{1,0:T(4,128)S(1)}, f32[3,64]{1,0:T(4,128)}, u32[]{:S(2)}) copy-start(f32[3,64]{1,0:T(4,128)} %param.17) | copy-start | bytes 2308
  157.4 21.7 %copy-start.9 = (f32[3]{0:T(128)S(1)}, f32[3]{0:T(128)}, u32[]{:S(2)}) copy-start(f32[3]{0:T(128)} %param.19) | copy-start | bytes 40
  157.4 165.8 %all-to-all-start.1 = ((bf16[16,96,2048]{2,1,0:T(8,128)(2,1)}), bf16[16,96,2048]{2,1,0:T(8,128)(2,1)}, u32[]{:S(2)}, u32[]{:S(2)}) async-start(bf16[16,96,2048]{2,1,0:T(8,128)(2,1)} %reshape.301), calls=%async_computation.2 | async-start | bytes 12582912 | tf_op jit(solution)/shard_map/all_to_all | solution.py:176
  174.0 178.1 %reduce-scatter.2.cloned.1.call-start = ((), (), s32[]{:S(2)}) async-start(), calls=%async_computation.4 | async-start | bytes 2228224 | tf_op jit(solution)/shard_map/reduce_scatter | solution.py:145
  174.2 4.4 %collective-permute-start = (bf16[2,128,1,64]{1,3,2,0:T(8,128)(2,1)S(1)}, bf16[2,128,1,64]{1,3,2,0:T(8,128)(2,1)S(1)}, u32[]{:S(2)}, u32[]{:S(2)}) collective-permute-start(bf16[2,128,1,64]{1,3,2,0:T(8,128)(2,1)S(1)} %pad_maximum_fusion.2), channel_id=1, source_target_pairs={{0,16},{16,32},{32,48},{48,64},{64,80},{80,96},{96,112},{112,128},... | collective-permute-start | bytes 98312 | tf_op jit(solution)/shard_map/ppermute | solution.py:38
  180.1 152.9 %copy-start.7 = (f32[32,2]{0,1:T(2,128)S(1)}, f32[32,2]{0,1:T(2,128)}, u32[]{:S(2)}) copy-start(f32[32,2]{0,1:T(2,128)} %param.24) | copy-start | bytes 772
  328.3 22.7 %all-to-all-start.2 = ((bf16[32,3,2048]{2,1,0:T(4,128)(2,1)}), bf16[32,3,2048]{2,1,0:T(4,128)(2,1)S(1)}, u32[]{:S(2)}, u32[]{:S(2)}) async-start(bf16[32,3,2048]{2,1,0:T(4,128)(2,1)} %reshape.302), calls=%async_computation.3 | async-start | bytes 1048576 | tf_op jit(solution)/shard_map/all_to_all | solution.py:179
Sparse Core Ops, SparseCore 0:
  182.3 132.2 reduce-scatter.1
